TPU v7x, 32 devices: a whole 2x2x4 slice. The times are simulated.
32 devices in a mesh: grp: 2 (over y), fs: 4 (over z), tp: 4 (over x, core).
Axes of the slice: x: 2, y: 2, z: 4, core: 2. Of those that a mesh axis runs over, the one named last changes fastest.
Arguments:
- layer_input_tokens: bfloat16 [4096, 2048], P(('grp', 'fs')), parts along dimension 0, may hold values from -6 to 6
- attention_norm_gain: float32 [2048], replicated, may hold values from 0.1 to 1.9
- query_projection: bfloat16 [2048, 1024], P('fs', 'tp'), may hold values from -0.125 to 0.125
- key_projection: bfloat16 [2048, 1024], P('fs', 'tp'), may hold values from -0.125 to 0.125
- value_projection: bfloat16 [2048, 2048], P('fs', 'tp'), may hold values from -0.125 to 0.125
- decay_first_factor: bfloat16 [2048, 16], replicated, may hold values from -0.125 to 0.125
- decay_second_factor: bfloat16 [16, 1024], P(None, 'tp'), may hold values from -1.5 to 1.5
- decay_logit_bias: float32 [1024], P('tp'), may hold values from -0.5 to 6
- extra_log_decay: float32 [4096, 8], P(('grp', 'fs'), 'tp'), parts along dimension 0, may hold values from -0.7 to 0
- head_output_gain: float32 [256], replicated, may hold values from 0.1 to 1.9
- attention_output_projection: bfloat16 [2048, 2048], P(('tp', 'fs')), may hold values from -0.125 to 0.125
- feedforward_norm_gain: float32 [2048], replicated, may hold values from 0.1 to 1.9
- gate_projection: bfloat16 [2048, 5632], P('fs', 'tp'), may hold values from -0.125 to 0.125
- up_projection: bfloat16 [2048, 5632], P('fs', 'tp'), may hold values from -0.125 to 0.125
- down_projection: bfloat16 [5632, 2048], P(('tp', 'fs')), may hold values from -0.078125 to 0.078125
Outputs:
- result: bfloat16 [4096, 2048], P(('grp', 'fs')), parts along dimension 0
There are 2 independent parts, one for each index of `grp`. A program takes and returns all parts, laid end to end along the dimension named above; an argument that names none is the same for every part. Nothing has to cross between parts.
All inputs are finite; a program needn't handle non-finite values.
Results may differ from a plain program's by a relative error of at most 0.02.
Values may be sent and summed in bfloat16 or wider, within the bound.
A program may use at most 64 MiB of HBM per device.

v0:
```python
import jax
import jax.numpy as jnp
from jax import lax
from jax.sharding import PartitionSpec as P

BLOCK = 64
normed_gate = 16.0


def norm_rows(values, gain):
    wide = values.astype(jnp.float32)
    scale = lax.rsqrt(jnp.mean(wide * wide, axis=-1, keepdims=True) + 1e-06)
    return wide * scale * gain


def block_scan(queries, keys, values, decays):
    length, key_channel_width = queries.shape
    value_width = values.shape[1]
    count = length // BLOCK
    lower_mask = jnp.arange(BLOCK)[:, None] >= jnp.arange(BLOCK)[None, :]

    def advance(carry, items):
        query_block, key_block, value_block, decay_block = items
        running = jnp.cumsum(decay_block, axis=0)
        middle = running[BLOCK // 2 - 1]
        closing = running[BLOCK - 1]
        carried = jnp.dot(query_block * jnp.exp(running), carry, precision=lax.Precision.HIGHEST)
        scores = jnp.dot(
            query_block * jnp.exp(running - middle),
            (key_block * jnp.exp(middle - running)).T,
            precision=lax.Precision.HIGHEST,
        )
        scores = jnp.where(lower_mask, scores, 0.0)
        inside = jnp.dot(scores, value_block, precision=lax.Precision.HIGHEST)
        fresh = carry * jnp.exp(closing)[:, None] + jnp.dot(
            (key_block * jnp.exp(closing - running)).T, value_block, precision=lax.Precision.HIGHEST
        )
        return (fresh, carried + inside)

    items = (
        queries.reshape(count, BLOCK, key_channel_width),
        keys.reshape(count, BLOCK, key_channel_width),
        values.reshape(count, BLOCK, value_width),
        decays.reshape(count, BLOCK, key_channel_width),
    )
    _, outputs = lax.scan(advance, jnp.zeros((key_channel_width, value_width), jnp.float32), items)
    return outputs.reshape(length, value_width)


def both_ways(queries, keys, values, decays):
    ahead = block_scan(queries, keys, values, decays)
    behind = block_scan(
        jnp.flip(queries, 0), jnp.flip(keys, 0), jnp.flip(values, 0), jnp.flip(decays, 0)
    )
    return ahead + jnp.flip(behind, 0)


def head_norm(mixed, gain):
    scale = lax.rsqrt(jnp.mean(mixed * mixed, axis=-1, keepdims=True) + 1e-06)
    return mixed * scale * gain


def shards(
    layer_input_tokens,
    attention_norm_gain,
    query_projection,
    key_projection,
    value_projection,
    decay_first_factor,
    decay_second_factor,
    decay_logit_bias,
    extra_log_decay,
    head_output_gain,
    attention_output_projection,
    feedforward_norm_gain,
    gate_projection,
    up_projection,
    down_projection,
):
    rows = layer_input_tokens.shape[0]
    normed = norm_rows(layer_input_tokens, attention_norm_gain).astype(jnp.bfloat16)
    pieces = (
        lax.all_gather(query_projection, "fs", axis=0, tiled=True),
        lax.all_gather(key_projection, "fs", axis=0, tiled=True),
        lax.all_gather(value_projection, "fs", axis=0, tiled=True),
    )
    query, key, value = tuple(
        (jnp.dot(normed, piece, preferred_element_type=jnp.float32) for piece in pieces)
    )
    query = query.astype(jnp.bfloat16)
    key = key.astype(jnp.bfloat16)
    value = value.astype(jnp.bfloat16)
    lowrank = jnp.dot(normed, decay_first_factor, preferred_element_type=jnp.float32).astype(
        jnp.bfloat16
    )
    decay_logit_values = (
        jnp.dot(lowrank, decay_second_factor, preferred_element_type=jnp.float32) + decay_logit_bias
    )
    local_heads = extra_log_decay.shape[1]
    key_channel_width = query.shape[1] // local_heads
    value_width = value.shape[1] // local_heads
    decay_logarithm = jax.nn.log_sigmoid(decay_logit_values) / normed_gate + jnp.repeat(
        extra_log_decay, key_channel_width, axis=1
    )
    mixed = jax.vmap(both_ways, in_axes=1, out_axes=1)(
        query.astype(jnp.float32).reshape(rows, local_heads, key_channel_width),
        key.astype(jnp.float32).reshape(rows, local_heads, key_channel_width),
        value.astype(jnp.float32).reshape(rows, local_heads, value_width),
        decay_logarithm.reshape(rows, local_heads, key_channel_width),
    )
    headed = (
        head_norm(mixed, head_output_gain)
        .reshape(rows, local_heads * value_width)
        .astype(jnp.bfloat16)
    )
    share = rows // lax.axis_size("tp")
    out_full = lax.all_gather(attention_output_projection, "fs", axis=0, tiled=True)
    mixer = lax.psum_scatter(
        jnp.dot(headed, out_full, preferred_element_type=jnp.float32).astype(jnp.bfloat16),
        "tp",
        scatter_dimension=0,
        tiled=True,
    ).astype(jnp.float32)
    own = lax.dynamic_slice_in_dim(layer_input_tokens, lax.axis_index("tp") * share, share, 0)
    residual = (own.astype(jnp.float32) + mixer).astype(jnp.bfloat16)
    second = lax.all_gather(
        norm_rows(residual, feedforward_norm_gain).astype(jnp.bfloat16), "tp", axis=0, tiled=True
    )
    gate_full, up_full = (
        lax.all_gather(gate_projection, "fs", axis=0, tiled=True),
        lax.all_gather(up_projection, "fs", axis=0, tiled=True),
    )
    gate = jnp.dot(second, gate_full, preferred_element_type=jnp.float32)
    up = jnp.dot(second, up_full, preferred_element_type=jnp.float32)
    hidden = (jax.nn.silu(gate) * up).astype(jnp.bfloat16)
    down_full = lax.all_gather(down_projection, "fs", axis=0, tiled=True)
    channel = lax.psum_scatter(
        jnp.dot(hidden, down_full, preferred_element_type=jnp.float32).astype(jnp.bfloat16),
        "tp",
        scatter_dimension=0,
        tiled=True,
    ).astype(jnp.float32)
    finished = (residual.astype(jnp.float32) + channel).astype(jnp.bfloat16)
    return lax.all_gather(finished, "tp", axis=0, tiled=True)


def solution(mesh):
    placed = (
        P(("grp", "fs"), None),
        P(),
        P("fs", "tp"),
        P("fs", "tp"),
        P("fs", "tp"),
        P(),
        P(None, "tp"),
        P("tp"),
        P(("grp", "fs"), "tp"),
        P(),
        P(("tp", "fs"), None),
        P(),
        P("fs", "tp"),
        P("fs", "tp"),
        P(("tp", "fs"), None),
    )
    return jax.shard_map(
        shards, mesh=mesh, in_specs=placed, out_specs=P(("grp", "fs"), None), check_vma=False
    )
```

profile of v0, /device:TPU:0, one launch (start us, length us, event | category | flops | bytes accessed | tf_op | source)
XLA Modules:
  0.0 674.9 jit_solution(432019829572898455)
XLA Ops:
  9.4 2.1 fusion.60
  11.6 2.0 fusion.74
  14.8 2.7 rev.18
  17.5 22.2 %all-gather.10.cloned.1.call-done = bf16[2048,256]{1,0:T(8,128)(2,1)} async-done(((bf16[512,256]{1,0:T(8,128)(2,1)}), bf16[2048,256]{1,0:T(8,128)(2,1)}) %all-gather.10.cloned.1.call-update) | async-done | bytes 1048592 | tf_op jit(solution)/shard_map/all_gather | solution.py:84
  39.7 2.1 convolution_convert_fusion.4
  42.0 2.6 rev.19
  44.6 24.1 %all-gather.14.cloned.1.call-done = bf16[2048,256]{1,0:T(8,128)(2,1)} async-done(((bf16[512,256]{1,0:T(8,128)(2,1)}), bf16[2048,256]{1,0:T(8,128)(2,1)}) %all-gather.14.cloned.1.call-update) | async-done | bytes 1048592 | tf_op jit(solution)/shard_map/all_gather | solution.py:83
  68.6 2.1 convolution_convert_fusion.3
  71.7 4.7 rev.21
  76.4 38.8 %all-gather.12.cloned.1.call-done = bf16[2048,512]{1,0:T(8,128)(2,1)} async-done(((bf16[512,512]{1,0:T(8,128)(2,1)}), bf16[2048,512]{1,0:T(8,128)(2,1)}) %all-gather.12.cloned.1.call-update) | async-done | bytes 2097168 | tf_op jit(solution)/shard_map/all_gather | solution.py:85
  115.3 3.8 convolution_convert_fusion.2
  120.3 5.1 rev.20
  126.5 51.9 %while.27 = (s32[]{:T(128)}, f32[2,128,256]{2,1,0:T(8,128)S(1)}, f32[8,2,64,256]{3,2,0,1:T(8,128)}, f32[8,2,64,128]{3,2,0,1:T(8,128)}, f32[8,2,64,128]{3,2,0,1:T...) while((s32[]{:T(128)}, f32[2,128,256]{2,1,0:T(8,128)S(1)}, ...), condition=%wide.region_6.7_spmd.clone, body=%wide.region_4.6_spmd.clone.sunk | while | flops 139866112 | bytes 2319992 | solution.py:46
  136.3 1.8 fusion.125
  142.8 1.8 fusion.125
  155.7 1.8 fusion.125
  162.2 1.8 fusion.125
  168.7 1.8 fusion.125
  178.6 31.7 %while.26 = (s32[]{:T(128)}, f32[2,128,256]{2,1,0:T(8,128)S(1)}, f32[8,2,64,256]{3,2,0,1:T(8,128)S(1)}, f32[8,2,64,128]{3,2,0,1:T(8,128)}, f32[8,2,64,128]{3,2,0...) while((s32[]{:T(128)}, f32[2,128,256]{2,1,0:T(8,128)S(1)}, ...), condition=%wide.region_3.4_spmd.clone, body=%wide.region_1.3_spmd.clone.sunk | while | flops 139866112 | bytes 2352760 | solution.py:46
  210.2 6.8 %rev.22 = f32[2,512,256]{2,1,0:T(8,128)S(1)} reverse(f32[2,512,256]{2,1,0:T(8,128)} %bitcast.196), dimensions={1} | reverse | bytes 2097152 | tf_op jit(solution)/shard_map/vmap(jit(_flip))/rev | solution.py:55
  217.9 4.2 convolution_convert_fusion
  222.8 29.6 %reduce-scatter.3.cloned.1.call-done = bf16[128,2048]{1,0:T(8,128)(2,1)} async-done(((bf16[512,2048]{1,0:T(8,128)(2,1)}), bf16[128,2048]{1,0:T(8,128)(2,1)}) %reduce-scatter.3.cloned.1.call-update) | async-done | bytes 524304 | tf_op jit(solution)/shard_map/reduce_scatter | solution.py:118
  256.6 103.9 %all-gather.20.cloned.1.call-done = bf16[2048,1408]{1,0:T(8,128)(2,1)} async-done(((bf16[512,1408]{1,0:T(8,128)(2,1)}), bf16[2048,1408]{1,0:T(8,128)(2,1)}) %all-gather.20.cloned.1.call-update) | async-done | bytes 5767184 | tf_op jit(solution)/shard_map/all_gather | solution.py:130
  360.5 22.4 %all-gather.18.cloned.1.call-done = bf16[512,2048]{1,0:T(8,128)(2,1)} async-done(((bf16[128,2048]{1,0:T(8,128)(2,1)}), bf16[512,2048]{1,0:T(8,128)(2,1)}) %all-gather.18.cloned.1.call-update) | async-done | bytes 2097168 | tf_op jit(solution)/shard_map/all_gather | solution.py:126
  382.9 8.4 %fusion.83 = f32[512,1408]{1,0:T(8,128)} fusion(bf16[512,2048]{1,0:T(8,128)(2,1)} %all-gather.18.cloned.1.call-done, bf16[2048,1408]{1,0:T(8,128)(2,1)} %all-gather.20.cloned.1.call-done), kind=kOutput, calls=%fused_computation.115 | convolution fusion | flops 2952790016 | bytes 10747904 | tf_op jit(solution)/shard_map/dot_general | solution.py:133
  391.3 99.9 %all-gather.22.cloned.1.call-done = bf16[2048,1408]{1,0:T(8,128)(2,1)} async-done(((bf16[512,1408]{1,0:T(8,128)(2,1)}), bf16[2048,1408]{1,0:T(8,128)(2,1)}) %all-gather.22.cloned.1.call-update) | async-done | bytes 5767184 | tf_op jit(solution)/shard_map/all_gather | solution.py:131
  491.2 106.6 %all-gather.24.cloned.1.call-done = bf16[1408,2048]{1,0:T(8,128)(2,1)} async-done(((bf16[352,2048]{1,0:T(8,128)(2,1)}), bf16[1408,2048]{1,0:T(8,128)(2,1)}) %all-gather.24.cloned.1.call-update) | async-done | bytes 5767184 | tf_op jit(solution)/shard_map/all_gather | solution.py:136
  597.8 13.2 %convolution_convert_fusion.1 = bf16[512,2048]{1,0:T(8,128)(2,1)} fusion(bf16[1408,2048]{1,0:T(8,128)(2,1)} %all-gather.24.cloned.1.call-done, bf16[512,2048]{1,0:T(8,128)(2,1)S(1)} %copy-done.9, bf16[2048,1408]{1,0:T(8,128)(2,1)} %all-gather.22.cloned.1.call-done, f32[512,1408]{1,0:T(8,128)} %fusion.83), kind=kOutput, calls=%fused_computation.84 | convolution fusion | flops 5910953984 | bytes 18612224 | tf_op jit(solution)/shard_map/dot_general | solution.py:138
  611.0 29.5 %reduce-scatter.5.cloned.1.call-done = bf16[128,2048]{1,0:T(8,128)(2,1)} async-done(((bf16[512,2048]{1,0:T(8,128)(2,1)}), bf16[128,2048]{1,0:T(8,128)(2,1)}) %reduce-scatter.5.cloned.1.call-update) | async-done | bytes 524304 | tf_op jit(solution)/shard_map/reduce_scatter | solution.py:137
  640.6 2.0 fusion.68
  642.6 22.7 %all-gather.26.cloned.1.call-done = bf16[512,2048]{1,0:T(8,128)(2,1)} async-done(((bf16[128,2048]{1,0:T(8,128)(2,1)}), bf16[512,2048]{1,0:T(8,128)(2,1)}) %all-gather.26.cloned.1.call-update) | async-done | bytes 2097168 | tf_op jit(solution)/shard_map/all_gather | solution.py:144
  665.3 3.2 copy.73
  (199 shorter events, 86.7 us)
Async XLA Ops:
  6.5 5.0 copy-start
  6.5 5.0 copy-start.1
  6.5 5.0 copy-start.4
  6.5 5.0 copy-start.3
  6.5 5.0 copy-start.7
  6.5 5.0 copy-start.6
  6.6 33.1 %all-gather.10.cloned.1.call-start = ((), (), s32[]{:S(2)}) async-start(), calls=%async_computation.2 | async-start | bytes 1310720 | tf_op jit(solution)/shard_map/all_gather | solution.py:84
  7.3 61.3 %all-gather.14.cloned.1.call-start = ((), (), s32[]{:S(2)}) async-start(), calls=%async_computation.4 | async-start | bytes 1310720 | tf_op jit(solution)/shard_map/all_gather | solution.py:83
  8.0 107.2 %all-gather.12.cloned.1.call-start = ((), (), s32[]{:S(2)}) async-start(), calls=%async_computation.3 | async-start | bytes 2621440 | tf_op jit(solution)/shard_map/all_gather | solution.py:85
  8.8 209.2 %all-gather.16.cloned.1.call-start = ((), (), s32[]{:S(2)}) async-start(), calls=%async_computation.5 | async-start | bytes 2621440 | tf_op jit(solution)/shard_map/all_gather | solution.py:117
  9.4 243.0 %reduce-scatter.3.cloned.1.call-start = ((), (), s32[]{:S(2)}) async-start(), calls=%async_computation.6 | async-start | bytes 2621440 | tf_op jit(solution)/shard_map/reduce_scatter | solution.py:118
  14.8 27.0 %copy-start.2 = (f32[512,2,128]{2,0,1:T(8,128)}, f32[512,2,128]{2,0,1:T(8,128)S(1)}, u32[]{:S(2)}) copy-start(f32[512,2,128]{2,0,1:T(8,128)S(1)} %copy.16) | copy-start | bytes 1572868
  210.2 7.2 %copy-start.8 = (f32[256]{0:T(256)S(1)}, f32[256]{0:T(256)}, u32[]{:S(2)}) copy-start(f32[256]{0:T(256)} %param.28) | copy-start | bytes 3076
  222.1 31.7 %copy-start.5 = (f32[2048]{0:T(1024)S(1)}, f32[2048]{0:T(1024)}, u32[]{:S(2)}) copy-start(f32[2048]{0:T(1024)} %param.30) | copy-start | bytes 24580
  222.2 138.3 %all-gather.20.cloned.1.call-start = ((), (), s32[]{:S(2)}) async-start(), calls=%async_computation.8 | async-start | bytes 7208960 | tf_op jit(solution)/shard_map/all_gather | solution.py:130
  222.7 160.2 %all-gather.18.cloned.1.call-start = ((), (), s32[]{:S(2)}) async-start(), calls=%async_computation.7 | async-start | bytes 2621440 | tf_op jit(solution)/shard_map/all_gather | solution.py:126
  254.8 236.4 %all-gather.22.cloned.1.call-start = ((), (), s32[]{:S(2)}) async-start(), calls=%async_computation.9 | async-start | bytes 7208960 | tf_op jit(solution)/shard_map/all_gather | solution.py:131
  255.6 342.2 %all-gather.24.cloned.1.call-start = ((), (), s32[]{:S(2)}) async-start(), calls=%async_computation.10 | async-start | bytes 7208960 | tf_op jit(solution)/shard_map/all_gather | solution.py:136
  256.3 384.2 %reduce-scatter.5.cloned.1.call-start = ((), (), s32[]{:S(2)}) async-start(), calls=%async_computation.11 | async-start | bytes 2621440 | tf_op jit(solution)/shard_map/reduce_scatter | solution.py:137
  382.9 214.8 %copy-start.9 = (bf16[512,2048]{1,0:T(8,128)(2,1)S(1)}, bf16[512,2048]{1,0:T(8,128)(2,1)}, u32[]{:S(2)}) copy-start(bf16[512,2048]{1,0:T(8,128)(2,1)} %all-gather.18.cloned.1.call-done) | copy-start | bytes 6291460
  611.0 54.3 %all-gather.26.cloned.1.call-start = ((), (), s32[]{:S(2)}) async-start(), calls=%async_computation.12 | async-start | bytes 2621440 | tf_op jit(solution)/shard_map/all_gather | solution.py:144
Sparse Core Ops, SparseCore 0:
  8.9 30.6 all-gather.9
  41.2 27.3 all-gather.13
  70.2 45.0 all-gather.11
  116.7 44.4 all-gather.15
  222.3 30.0 reduce-scatter.2
  253.8 106.6 all-gather.19
  362.1 20.8 all-gather.17
  384.5 106.6 all-gather.21
  492.8 104.9 all-gather.23
  611.1 29.4 reduce-scatter.4
  642.7 22.5 all-gather.25
where the time goes:
time: 679 us; the launch traced here: 675 us
  waiting for transfers between devices  504 us (74%)
  matrix products  103 us (15%)
  local copies, waits for them, and re-layouts  43.9 us (6%)
  between operations  13.5 us (2%)
  other arithmetic  8.82 us (1%)
    all_gather x1, waiting for transfers between devices, shards(): down_full = lax.all_gather(down_projection, 'fs', axis=0, tiled=True)  107 us
    all_gather x1, waiting for transfers between devices, shards(): lax.all_gather(gate_projection, 'fs', axis=0, tiled=True)  104 us
    all_gather x1, waiting for transfers between devices, shards(): lax.all_gather(up_projection, 'fs', axis=0, tiled=True)  99.9 us
    all_gather x1, waiting for transfers between devices, shards(): lax.all_gather(value_projection, 'fs', axis=0, tiled=True)  38.8 us
    reduce_scatter x1, waiting for transfers between devices, shards(): lax.psum_scatter(jnp.dot(headed, out_full, preferred_element_type=jnp.flo...  29.6 us
    reduce_scatter x1, waiting for transfers between devices, shards(): lax.psum_scatter(jnp.dot(hidden, down_full, preferred_element_type=jnp.fl...  29.5 us
    all_gather x1, waiting for transfers between devices, shards(): lax.all_gather(query_projection, 'fs', axis=0, tiled=True)  24.1 us
    all_gather x1, waiting for transfers between devices, shards(): return lax.all_gather(finished, 'tp', axis=0, tiled=True)  22.7 us
  transfers between devices with their start and end apart: 11, of which 10 were waited for; matrix products, arithmetic and copies ran while one was open for 20% of the time, Pallas kernels for 0%

commit v1 on v0

--- a/solution.py
+++ b/solution.py
@@ -133,7 +133,13 @@
     gate = jnp.dot(second, gate_full, preferred_element_type=jnp.float32)
     up = jnp.dot(second, up_full, preferred_element_type=jnp.float32)
     hidden = (jax.nn.silu(gate) * up).astype(jnp.bfloat16)
-    down_full = lax.all_gather(down_projection, "fs", axis=0, tiled=True)
+    peers = lax.axis_size("fs")
+    current, parts = (down_projection, [down_projection])
+    for _ in range(peers - 1):
+        current = lax.ppermute(current, "fs", [(i, (i + 1) % peers) for i in range(peers)])
+        parts.insert(0, current)
+    line = jnp.concatenate(parts, axis=0)
+    down_full = jnp.roll(line, (lax.axis_index("fs") + 1) * down_projection.shape[0], axis=0)
     channel = lax.psum_scatter(
         jnp.dot(hidden, down_full, preferred_element_type=jnp.float32).astype(jnp.bfloat16),
         "tp",

time: 679 us -> 626 us (0.922)
  waiting for transfers between devices: 504 us -> 399 us
  starting transfers between devices: 0.61 us -> 37.1 us
  local copies, waits for them, and re-layouts: 43.9 us -> 59.5 us
    ppermute x0 -> x3, waiting for transfers between devices: none -> 154 us  [shards(): lax.ppermute(current, 'fs', [(i, (i + 1) % peers) for i in range(peers)])]
    all_gather x1 -> x0, waiting for transfers between devices: 107 us -> none  [shards(): down_full = lax.all_gather(down_projection, 'fs', axis=0, tiled=True)]
    all_gather x1, waiting for transfers between devices: 104 us -> 0.01 us  [shards(): lax.all_gather(gate_projection, 'fs', axis=0, tiled=True)]
    ppermute x0 -> x3, starting transfers between devices: none -> 36.7 us  [shards(): lax.ppermute(current, 'fs', [(i, (i + 1) % peers) for i in range(peers)])]
    all_gather x1, waiting for transfers between devices: 99.9 us -> 73.9 us  [shards(): lax.all_gather(up_projection, 'fs', axis=0, tiled=True)]
    all_gather x1, waiting for transfers between devices: 22.4 us -> 0.01 us  [shards(): lax.all_gather(norm_rows(residual, feedforward_norm_gain).astype(jnp.bflo...]
    unnamed x21 -> x30, local copies, waits for them, and re-layouts: 3.2 us -> 17.5 us
  transfers between devices with their start and end apart: 11 -> 13, of which waited for: 10 -> 10; matrix products, arithmetic and copies ran while one was open for 20% -> 24% of each run, Pallas kernels for 0% -> 0%
where the time goes in v1:
time: 626 us; the launch traced here: 623 us
  waiting for transfers between devices  399 us (64%)
  matrix products  104 us (17%)
  local copies, waits for them, and re-layouts  59.5 us (10%)
  starting transfers between devices  37.1 us (6%)
  between operations  13.8 us (2%)
  other arithmetic  8.82 us (1%)
    ppermute x3, waiting for transfers between devices, shards(): lax.ppermute(current, 'fs', [(i, (i + 1) % peers) for i in range(peers)])  154 us
    all_gather x1, waiting for transfers between devices, shards(): lax.all_gather(up_projection, 'fs', axis=0, tiled=True)  73.9 us
    all_gather x1, waiting for transfers between devices, shards(): lax.all_gather(value_projection, 'fs', axis=0, tiled=True)  38.8 us
    ppermute x3, starting transfers between devices, shards(): lax.ppermute(current, 'fs', [(i, (i + 1) % peers) for i in range(peers)])  36.7 us
    reduce_scatter x1, waiting for transfers between devices, shards(): lax.psum_scatter(jnp.dot(headed, out_full, preferred_element_type=jnp.flo...  29.5 us
    reduce_scatter x1, waiting for transfers between devices, shards(): lax.psum_scatter(jnp.dot(hidden, down_full, preferred_element_type=jnp.fl...  29.5 us
    all_gather x1, waiting for transfers between devices, shards(): lax.all_gather(query_projection, 'fs', axis=0, tiled=True)  24 us
    all_gather x1, waiting for transfers between devices, shards(): return lax.all_gather(finished, 'tp', axis=0, tiled=True)  22.7 us
  transfers between devices with their start and end apart: 13, of which 10 were waited for; matrix products, arithmetic and copies ran while one was open for 24% of the time, Pallas kernels for 0%

profile of v1, /device:TPU:0, one launch (start us, length us, event | category | flops | bytes accessed | tf_op | source)
XLA Modules:
  0.0 622.7 jit_solution(5781928985703378375)
XLA Ops:
  9.4 2.1 fusion.62
  11.6 2.0 fusion.79
  14.8 2.7 rev.18
  17.5 22.1 %all-gather.9.cloned.1.call-done = bf16[2048,256]{1,0:T(8,128)(2,1)} async-done(((bf16[512,256]{1,0:T(8,128)(2,1)}), bf16[2048,256]{1,0:T(8,128)(2,1)}) %all-gather.9.cloned.1.call-update) | async-done | bytes 1048592 | tf_op jit(solution)/shard_map/all_gather | solution.py:84
  39.7 2.1 convolution_convert_fusion.3
  42.0 2.6 rev.19
  44.6 24.0 %all-gather.13.cloned.1.call-done = bf16[2048,256]{1,0:T(8,128)(2,1)} async-done(((bf16[512,256]{1,0:T(8,128)(2,1)}), bf16[2048,256]{1,0:T(8,128)(2,1)}) %all-gather.13.cloned.1.call-update) | async-done | bytes 1048592 | tf_op jit(solution)/shard_map/all_gather | solution.py:83
  68.6 2.1 convolution_convert_fusion.2
  71.7 4.7 rev.21
  76.5 38.8 %all-gather.11.cloned.1.call-done = bf16[2048,512]{1,0:T(8,128)(2,1)} async-done(((bf16[512,512]{1,0:T(8,128)(2,1)}), bf16[2048,512]{1,0:T(8,128)(2,1)}) %all-gather.11.cloned.1.call-update) | async-done | bytes 2097168 | tf_op jit(solution)/shard_map/all_gather | solution.py:85
  115.3 3.8 convolution_convert_fusion.1
  120.3 5.2 rev.20
  126.5 51.8 %while.27 = (s32[]{:T(128)}, f32[2,128,256]{2,1,0:T(8,128)S(1)}, f32[8,2,64,256]{3,2,0,1:T(8,128)}, f32[8,2,64,128]{3,2,0,1:T(8,128)}, f32[8,2,64,128]{3,2,0,1:T...) while((s32[]{:T(128)}, f32[2,128,256]{2,1,0:T(8,128)S(1)}, ...), condition=%wide.region_6.7_spmd.clone, body=%wide.region_4.6_spmd.clone.sunk | while | flops 139866112 | bytes 2320003 | solution.py:46
  178.5 31.7 %while.26 = (s32[]{:T(128)}, f32[2,128,256]{2,1,0:T(8,128)S(1)}, f32[8,2,64,256]{3,2,0,1:T(8,128)S(1)}, f32[8,2,64,128]{3,2,0,1:T(8,128)}, f32[8,2,64,128]{3,2,0...) while((s32[]{:T(128)}, f32[2,128,256]{2,1,0:T(8,128)S(1)}, ...), condition=%wide.region_3.4_spmd.clone, body=%wide.region_1.3_spmd.clone.sunk | while | flops 139866112 | bytes 2352771 | solution.py:46
  210.2 6.8 %rev.22 = f32[2,512,256]{2,1,0:T(8,128)S(1)} reverse(f32[2,512,256]{2,1,0:T(8,128)} %bitcast.195), dimensions={1} | reverse | bytes 2097152 | tf_op jit(solution)/shard_map/vmap(jit(_flip))/rev | solution.py:55
  217.9 4.2 convolution_convert_fusion
  222.7 29.5 %reduce-scatter.3.cloned.1.call-done = bf16[128,2048]{1,0:T(8,128)(2,1)} async-done(((bf16[512,2048]{1,0:T(8,128)(2,1)}), bf16[128,2048]{1,0:T(8,128)(2,1)}) %reduce-scatter.3.cloned.1.call-update) | async-done | bytes 524304 | tf_op jit(solution)/shard_map/reduce_scatter | solution.py:118
  257.1 58.4 %collective-permute-done = bf16[352,2048]{1,0:T(8,128)(2,1)S(1)} collective-permute-done((bf16[352,2048]{1,0:T(8,128)(2,1)S(1)}, bf16[352,2048]{1,0:T(8,128)(2,1)S(1)}, u32[]{:S(2)}, u32[]{:S(2)}) %collective-permute-start) | collective-permute-done | bytes 1441824 | tf_op jit(solution)/shard_map/ppermute | solution.py:139
  315.5 27.0 %collective-permute-start.1 = (bf16[352,2048]{1,0:T(8,128)(2,1)S(1)}, bf16[352,2048]{1,0:T(8,128)(2,1)}, u32[]{:S(2)}, u32[]{:S(2)}) collective-permute-start(bf16[352,2048]{1,0:T(8,128)(2,1)S(1)} %collective-permute-done), channel_id=1, source_target_pairs={{0,4},{4,8},{8,12},{12,0},{1,5},{5,9},{9,13},{13,1},{2,6},{6,10},{... | collective-permute-start | bytes 4325384 | tf_op jit(solution)/shard_map/ppermute | solution.py:139
  342.6 62.2 %collective-permute-done.1 = bf16[352,2048]{1,0:T(8,128)(2,1)} collective-permute-done((bf16[352,2048]{1,0:T(8,128)(2,1)S(1)}, bf16[352,2048]{1,0:T(8,128)(2,1)}, u32[]{:S(2)}, u32[]{:S(2)}) %collective-permute-start.1) | collective-permute-done | bytes 1441824 | tf_op jit(solution)/shard_map/ppermute | solution.py:139
  404.8 8.1 %collective-permute-start.2 = (bf16[352,2048]{1,0:T(8,128)(2,1)}, bf16[352,2048]{1,0:T(8,128)(2,1)}, u32[]{:S(2)}, u32[]{:S(2)}) collective-permute-start(bf16[352,2048]{1,0:T(8,128)(2,1)} %collective-permute-done.1), channel_id=1, source_target_pairs={{0,4},{4,8},{8,12},{12,0},{1,5},{5,9},{9,13},{13,1},{2,6},{6,10},{... | collective-permute-start | bytes 4325384 | tf_op jit(solution)/shard_map/ppermute | solution.py:139
  412.9 33.8 %collective-permute-done.2 = bf16[352,2048]{1,0:T(8,128)(2,1)} collective-permute-done((bf16[352,2048]{1,0:T(8,128)(2,1)}, bf16[352,2048]{1,0:T(8,128)(2,1)}, u32[]{:S(2)}, u32[]{:S(2)}) %collective-permute-start.2) | collective-permute-done | bytes 1441824 | tf_op jit(solution)/shard_map/ppermute | solution.py:139
  446.6 2.7 constant_dynamic-update-slice_fusion.7
  449.3 2.6 constant_dynamic-update-slice_fusion.6
  454.4 2.6 constant_dynamic-update-slice_fusion.3
  457.1 2.7 constant_dynamic-update-slice_fusion.2
  462.2 8.4 %fusion.89 = f32[512,1408]{1,0:T(8,128)} fusion(bf16[512,2048]{1,0:T(8,128)(2,1)} %all-gather.17.cloned.1.call-done, bf16[2048,1408]{1,0:T(8,128)(2,1)} %all-gather.19.cloned.1.call-done), kind=kOutput, calls=%fused_computation.126 | convolution fusion | flops 2952790016 | bytes 10747904 | tf_op jit(solution)/shard_map/dot_general | solution.py:133
  470.5 73.9 %all-gather.21.cloned.1.call-done = bf16[2048,1408]{1,0:T(8,128)(2,1)} async-done(((bf16[512,1408]{1,0:T(8,128)(2,1)}), bf16[2048,1408]{1,0:T(8,128)(2,1)}) %all-gather.21.cloned.1.call-update) | async-done | bytes 5767184 | tf_op jit(solution)/shard_map/all_gather | solution.py:131
  544.4 14.0 %fusion.66 = bf16[512,2048]{1,0:T(8,128)(2,1)} fusion(bf16[2816,2048]{1,0:T(8,128)(2,1)} %constant_dynamic-update-slice_fusion, s32[]{:T(128)S(6)} %select_n.31, bf16[512,2048]{1,0:T(8,128)(2,1)} %all-gather.17.cloned.1.call-done, bf16[2048,1408]{1,0:T(8,128)(2,1)} %all-gather.21.cloned.1.call-done, f32[512,1408]{1,0:T(8,128)} %fusion.89), kind=kOutput, calls=%fused_computation.85 | convolution fusion | flops 5910953984 | bytes 18612228 | tf_op jit(solution)/shard_map/dot_general | solution.py:144
  558.5 29.5 %reduce-scatter.5.cloned.1.call-done = bf16[128,2048]{1,0:T(8,128)(2,1)} async-done(((bf16[512,2048]{1,0:T(8,128)(2,1)}), bf16[128,2048]{1,0:T(8,128)(2,1)}) %reduce-scatter.5.cloned.1.call-update) | async-done | bytes 524304 | tf_op jit(solution)/shard_map/reduce_scatter | solution.py:143
  590.0 22.7 %all-gather.23.cloned.1.call-done = bf16[512,2048]{1,0:T(8,128)(2,1)} async-done(((bf16[128,2048]{1,0:T(8,128)(2,1)}), bf16[512,2048]{1,0:T(8,128)(2,1)}) %all-gather.23.cloned.1.call-update) | async-done | bytes 2097168 | tf_op jit(solution)/shard_map/all_gather | solution.py:150
  612.7 3.2 copy.80
  (212 shorter events, 103.2 us)
Async XLA Ops:
  6.5 5.0 copy-start
  6.5 5.0 copy-start.2
  6.5 5.0 copy-start.5
  6.5 5.0 copy-start.8
  6.5 5.0 copy-start.9
  6.5 5.0 copy-start.6
  6.6 33.1 %all-gather.9.cloned.1.call-start = ((), (), s32[]{:S(2)}) async-start(), calls=%async_computation.2 | async-start | bytes 1310720 | tf_op jit(solution)/shard_map/all_gather | solution.py:84
  7.3 61.3 %all-gather.13.cloned.1.call-start = ((), (), s32[]{:S(2)}) async-start(), calls=%async_computation.4 | async-start | bytes 1310720 | tf_op jit(solution)/shard_map/all_gather | solution.py:83
  8.0 107.2 %all-gather.11.cloned.1.call-start = ((), (), s32[]{:S(2)}) async-start(), calls=%async_computation.3 | async-start | bytes 2621440 | tf_op jit(solution)/shard_map/all_gather | solution.py:85
  8.8 209.1 %all-gather.15.cloned.1.call-start = ((), (), s32[]{:S(2)}) async-start(), calls=%async_computation.5 | async-start | bytes 2621440 | tf_op jit(solution)/shard_map/all_gather | solution.py:117
  9.4 242.9 %reduce-scatter.3.cloned.1.call-start = ((), (), s32[]{:S(2)}) async-start(), calls=%async_computation.6 | async-start | bytes 2621440 | tf_op jit(solution)/shard_map/reduce_scatter | solution.py:118
  14.8 27.0 %copy-start.4 = (f32[512,2,128]{2,0,1:T(8,128)}, f32[512,2,128]{2,0,1:T(8,128)S(1)}, u32[]{:S(2)}) copy-start(f32[512,2,128]{2,0,1:T(8,128)S(1)} %copy.16) | copy-start | bytes 1572868
  210.2 7.2 %copy-start.10 = (f32[256]{0:T(256)S(1)}, f32[256]{0:T(256)}, u32[]{:S(2)}) copy-start(f32[256]{0:T(256)} %param.28) | copy-start | bytes 3076
  222.1 31.7 %copy-start.7 = (f32[2048]{0:T(1024)S(1)}, f32[2048]{0:T(1024)}, u32[]{:S(2)}) copy-start(f32[2048]{0:T(1024)} %param.30) | copy-start | bytes 24580
  222.1 33.5 %copy-start.3 = (bf16[352,2048]{1,0:T(8,128)(2,1)S(1)}, bf16[352,2048]{1,0:T(8,128)(2,1)}, u32[]{:S(2)}) copy-start(bf16[352,2048]{1,0:T(8,128)(2,1)} %param.33) | copy-start | bytes 4325380
  222.1 240.1 %all-gather.19.cloned.1.call-start = ((), (), s32[]{:S(2)}) async-start(), calls=%async_computation.8 | async-start | bytes 7208960 | tf_op jit(solution)/shard_map/all_gather | solution.py:130
  222.7 239.5 %all-gather.17.cloned.1.call-start = ((), (), s32[]{:S(2)}) async-start(), calls=%async_computation.7 | async-start | bytes 2621440 | tf_op jit(solution)/shard_map/all_gather | solution.py:126
  254.7 289.7 %all-gather.21.cloned.1.call-start = ((), (), s32[]{:S(2)}) async-start(), calls=%async_computation.9 | async-start | bytes 7208960 | tf_op jit(solution)/shard_map/all_gather | solution.py:131
  255.5 332.5 %reduce-scatter.5.cloned.1.call-start = ((), (), s32[]{:S(2)}) async-start(), calls=%async_computation.10 | async-start | bytes 2621440 | tf_op jit(solution)/shard_map/reduce_scatter | solution.py:143
  255.6 60.0 %collective-permute-start = (bf16[352,2048]{1,0:T(8,128)(2,1)S(1)}, bf16[352,2048]{1,0:T(8,128)(2,1)S(1)}, u32[]{:S(2)}, u32[]{:S(2)}) collective-permute-start(bf16[352,2048]{1,0:T(8,128)(2,1)S(1)} %copy-done.3), channel_id=1, source_target_pairs={{0,4},{4,8},{8,12},{12,0},{1,5},{5,9},{9,13},{13,1},{2,6},{6,10},{... | collective-permute-start | bytes 4325384 | tf_op jit(solution)/shard_map/ppermute | solution.py:139
  315.5 89.3 %collective-permute-start.1 = (bf16[352,2048]{1,0:T(8,128)(2,1)S(1)}, bf16[352,2048]{1,0:T(8,128)(2,1)}, u32[]{:S(2)}, u32[]{:S(2)}) collective-permute-start(bf16[352,2048]{1,0:T(8,128)(2,1)S(1)} %collective-permute-done), channel_id=1, source_target_pairs={{0,4},{4,8},{8,12},{12,0},{1,5},{5,9},{9,13},{13,1},{2,6},{6,10},{... | collective-permute-start | bytes 4325384 | tf_op jit(solution)/shard_map/ppermute | solution.py:139
  404.8 41.9 %collective-permute-start.2 = (bf16[352,2048]{1,0:T(8,128)(2,1)}, bf16[352,2048]{1,0:T(8,128)(2,1)}, u32[]{:S(2)}, u32[]{:S(2)}) collective-permute-start(bf16[352,2048]{1,0:T(8,128)(2,1)} %collective-permute-done.1), channel_id=1, source_target_pairs={{0,4},{4,8},{8,12},{12,0},{1,5},{5,9},{9,13},{13,1},{2,6},{6,10},{... | collective-permute-start | bytes 4325384 | tf_op jit(solution)/shard_map/ppermute | solution.py:139
  558.4 57.4 %copy-start.1 = (bf16[2048,16]{0,1:T(8,128)(2,1)S(1)}, bf16[2048,16]{0,1:T(8,128)(2,1)}, u32[]{:S(2)}) copy-start(bf16[2048,16]{0,1:T(8,128)(2,1)} %param.24) | copy-start | bytes 196612
  558.5 54.2 %all-gather.23.cloned.1.call-start = ((), (), s32[]{:S(2)}) async-start(), calls=%async_computation.11 | async-start | bytes 2621440 | tf_op jit(solution)/shard_map/all_gather | solution.py:150
Sparse Core Ops, SparseCore 0:
  8.9 30.6 all-gather.8
  41.2 27.3 all-gather.12
  70.2 45.0 all-gather.10
  116.7 44.5 all-gather.14
  222.2 29.9 reduce-scatter.2
  253.7 160.9 all-gather.18
  416.3 19.8 all-gather.16
  437.7 106.6 all-gather.20
  558.6 29.3 reduce-scatter.4
  590.1 22.5 all-gather.22
